TPU v7x, 32 devices: a whole 2x2x4 slice. The times are simulated.
32 devices in a mesh: fs: 4 (over z), rep: 4 (over y, x), tp: 2 (over core).
Axes of the slice: x: 2, y: 2, z: 4, core: 2. Of those that a mesh axis runs over, the one named last changes fastest.
Arguments:
- saved_input: bfloat16 [16384, 2048], P(('fs', 'rep')), may hold values from -6 to 6
- value_cotangent: bfloat16 [16384, 4096], P(('fs', 'rep'), 'tp'), may hold values from -0.0061950684 to 0.0061950684
- factor: bfloat16 [2048, 128], P('fs'), may hold values from -1.5 to 1.5
- weight: float32 [2048, 4096], P('fs', 'tp'), may hold values from -1.2 to 1.2
- first_moment: float32 [128, 4096], P('fs', 'tp'), may hold values from -1.8 to 1.8
- second_moment: float32 [128, 4096], P('fs', 'tp'), may hold values from 0.1 to 1
Outputs:
- low_grad: float32 [128, 4096], P('fs', 'tp')
- new_first: float32 [128, 4096], P('fs', 'tp')
- new_second: float32 [128, 4096], P('fs', 'tp')
- direction: float32 [2048, 4096], P('fs', 'tp')
- new_weight: float32 [2048, 4096], P('fs', 'tp')
- new_copy: bfloat16 [2048, 4096], P('fs', 'tp')
All inputs are finite; a program needn't handle non-finite values.
Results may differ from a plain program's by a relative error of at most 0.006.
Values may be sent and summed in bfloat16 or wider, within the bound.
A program may use at most 64 MiB of HBM per device.

v0:
```python
import jax
import jax.numpy as jnp
from jax import lax
from jax.sharding import PartitionSpec as P

D = 2048
E = 4096
first_decay = 0.9
second_decay = 0.9
learn_rate = 0.05
epsilon = 1e-08


def on_device(saved_input, value_cotangent, factor, weight, first_moment, second_moment):
    factor_wide = factor.astype(jnp.float32)
    factor_whole = lax.all_gather(factor, "fs", axis=0, tiled=True)
    projected = jnp.dot(saved_input, factor_whole, preferred_element_type=jnp.float32)
    upper = projected.astype(jnp.bfloat16)
    lower = (projected - upper.astype(jnp.float32)).astype(jnp.bfloat16)
    dims = (((0,), (0,)), ((), ()))
    high_part = lax.dot_general(upper, value_cotangent, dims, preferred_element_type=jnp.float32)
    low_part = lax.dot_general(lower, value_cotangent, dims, preferred_element_type=jnp.float32)
    low_grad = lax.psum_scatter(high_part + low_part, "fs", scatter_dimension=0, tiled=True)
    low_grad = lax.psum(low_grad, "rep")
    new_first = first_decay * first_moment + (1.0 - first_decay) * low_grad
    new_second = second_decay * second_moment + (1.0 - second_decay) * low_grad * low_grad
    ratio = new_first / (jnp.sqrt(new_second) + epsilon)
    ratio_whole = lax.all_gather(ratio, "fs", axis=0, tiled=True)
    raw = jnp.dot(factor_wide, ratio_whole, precision=lax.Precision.HIGHEST)
    total = lax.psum(jnp.sum(raw * raw), ("fs", "tp"))
    spread = jnp.sqrt(total / (D * E))
    direction = raw / (spread + 1.0)
    new_weight = weight - learn_rate * direction
    return (low_grad, new_first, new_second, direction, new_weight, new_weight.astype(jnp.bfloat16))


def solution(mesh):
    placed = (
        P(("fs", "rep"), None),
        P(("fs", "rep"), "tp"),
        P("fs", None),
        P("fs", "tp"),
        P("fs", "tp"),
        P("fs", "tp"),
    )
    return jax.shard_map(
        on_device,
        mesh=mesh,
        in_specs=placed,
        out_specs=(
            P("fs", "tp"),
            P("fs", "tp"),
            P("fs", "tp"),
            P("fs", "tp"),
            P("fs", "tp"),
            P("fs", "tp"),
        ),
        check_vma=False,
    )
```

profile of v0, /device:TPU:0, one launch (start us, length us, event | category | flops | bytes accessed | tf_op | source)
XLA Modules:
  0.0 185.3 jit_solution(11213346444921834174)
XLA Ops:
  7.2 0.0 reduce-scatter.2.cloned.1.call-start
  7.2 0.0 copy-start
  7.2 17.7 %all_gather.6 = bf16[2048,128]{1,0:T(8,128)(2,1)S(1)} all-gather(bf16[512,128]{1,0:T(8,128)(2,1)} %param.8), channel_id=1, replica_groups=mesh['fs'=4,'rep'=4,'tp'=2] {'fs'}, dimensions={0}, use_global_device_ids=true | all-gather | bytes 655360 | tf_op jit(solution)/shard_map/all_gather | solution.py:16
  24.9 3.4 %fusion.6 = f32[1024,128]{1,0:T(8,128)S(1)} fusion(bf16[1024,2048]{1,0:T(8,128)(2,1)} %param.6, bf16[2048,128]{1,0:T(8,128)(2,1)S(1)} %all_gather.6), kind=kOutput, calls=%fused_computation.13 | convolution fusion | flops 536870912 | bytes 5242880 | tf_op jit(solution)/shard_map/dot_general | solution.py:17
  28.4 0.0 copy-done
  28.4 0.7 fusion.2
  29.1 0.0 copy-start.3
  29.1 0.0 copy-start.4
  29.2 1.7 convolution_add_fusion
  30.9 0.0 reduce-scatter.2.cloned.1.call-update
  30.9 0.0 all-reduce.2.cloned.1.call-start
  31.0 29.2 %reduce-scatter.2.cloned.1.call-done = f32[32,2048]{1,0:T(8,128)} async-done(((f32[128,2048]{1,0:T(8,128)}), f32[32,2048]{1,0:T(8,128)}) %reduce-scatter.2.cloned.1.call-update) | async-done | bytes 262160 | tf_op jit(solution)/shard_map/reduce_scatter | solution.py:23
  60.1 0.0 all-reduce.2.cloned.1.call-update
  60.1 0.0 all-gather.2.cloned.1.call-start
  60.2 44.5 %all-reduce.2.cloned.1.call-done = f32[32,2048]{1,0:T(8,128)} async-done(((f32[32,2048]{1,0:T(8,128)}), f32[32,2048]{1,0:T(8,128)}) %all-reduce.2.cloned.1.call-update) | async-done | bytes 262160 | tf_op jit(solution)/shard_map/psum | solution.py:24
  104.6 0.0 copy-done.3
  104.6 0.0 copy-done.4
  104.6 1.9 %add_divide_fusion = (f32[32,2048]{1,0:T(8,128)}, f32[32,2048]{1,0:T(8,128)}, f32[32,2048]{1,0:T(8,128)}) fusion(f32[32,2048]{1,0:T(8,128)} %all-reduce.2.cloned.1.call-done, f32[32,2048]{1,0:T(8,128)S(1)} %copy-done.3, f32[32,2048]{1,0:T(8,128)S(1)} %copy-done.4), kind=kLoop, calls=%fused_computation.8 | loop fusion | flops 524288 | bytes 1572864 | tf_op jit(solution)/shard_map/div | solution.py:27
  106.5 0.0 all-gather.2.cloned.1.call-update
  106.6 0.0 copy-start.2
  106.6 5.4 %copy.12 = f32[512,2048]{0,1:T(8,128)} copy(f32[512,2048]{1,0:T(8,128)} %param.9) | data formatting | bytes 8388608 | tf_op args[3]
  112.0 22.8 %all-gather.2.cloned.1.call-done = f32[128,2048]{1,0:T(8,128)} async-done(((f32[32,2048]{1,0:T(8,128)}), f32[128,2048]{1,0:T(8,128)}) %all-gather.2.cloned.1.call-update) | async-done | bytes 1048592 | tf_op jit(solution)/shard_map/all_gather | solution.py:28
  134.8 0.0 copy-done.2
  134.8 6.0 %multiply_reduce_fusion = (f32[]{:T(128)}, f32[2048,512]{1,0:T(8,128)}) fusion(f32[128,2048]{1,0:T(8,128)} %all-gather.2.cloned.1.call-done, bf16[512,128]{1,0:T(8,128)(2,1)S(1)} %copy-done.2), kind=kOutput, calls=%fused_computation.2 | convolution fusion | flops 1612709888 | bytes 5373956 | tf_op jit(solution)/shard_map/dot_general | solution.py:29
  140.8 15.3 %psum.15 = f32[]{:T(128)} all-reduce(f32[]{:T(128)} %get-tuple-element.18), channel_id=1, replica_groups=mesh['fs'=4,'rep'=4,'tp'=2] {'fs','tp'}, use_global_device_ids=true, to_apply=%region_3.0 | all-reduce | flops 1 | bytes 8 | tf_op jit(solution)/shard_map/psum | solution.py:30
  156.7 8.3 %fusion.4 = (bf16[512,2048]{0,1:T(8,128)(2,1)S(1)}, f32[512,2048]{0,1:T(8,128)}, f32[512,2048]{0,1:T(8,128)}) fusion(f32[512,2048]{0,1:T(8,128)} %copy.12, f32[2048,512]{1,0:T(8,128)} %get-tuple-element.19, f32[]{:T(128)S(6)} %add.29), kind=kLoop, calls=%fused_computation.12 | loop fusion | flops 4194304 | bytes 18874372 | tf_op jit(solution)/shard_map/convert_element_type | solution.py:34
  165.0 2.4 %copy.15 = bf16[512,2048]{1,0:T(8,128)(2,1)} copy(bf16[512,2048]{0,1:T(8,128)(2,1)S(1)} %get-tuple-element.12) | data formatting | bytes 4194304
  167.4 5.3 %copy.14 = f32[512,2048]{1,0:T(8,128)} copy(f32[512,2048]{0,1:T(8,128)} %get-tuple-element.13) | data formatting | bytes 8388608
  172.7 0.0 copy-start.1
  172.7 5.4 %copy.13 = f32[512,2048]{1,0:T(8,128)} copy(f32[512,2048]{0,1:T(8,128)} %get-tuple-element.14) | data formatting | bytes 8388608
  178.1 0.0 copy-done.1
  178.1 0.7 copy.17
Async XLA Ops:
  7.2 52.9 %reduce-scatter.2.cloned.1.call-start = ((), (), s32[]{:S(2)}) async-start(), calls=%async_computation.1 | async-start | bytes 1310720 | tf_op jit(solution)/shard_map/reduce_scatter | solution.py:23
  7.2 21.2 %copy-start = (bf16[1024,2048]{1,0:T(8,128)(2,1)S(1)}, bf16[1024,2048]{1,0:T(8,128)(2,1)}, u32[]{:S(2)}) copy-start(bf16[1024,2048]{1,0:T(8,128)(2,1)} %param.7) | copy-start | bytes 12582916
  29.1 75.5 %copy-start.3 = (f32[32,2048]{1,0:T(8,128)S(1)}, f32[32,2048]{1,0:T(8,128)}, u32[]{:S(2)}) copy-start(f32[32,2048]{1,0:T(8,128)} %param.11) | copy-start | bytes 786436
  29.1 75.5 %copy-start.4 = (f32[32,2048]{1,0:T(8,128)S(1)}, f32[32,2048]{1,0:T(8,128)}, u32[]{:S(2)}) copy-start(f32[32,2048]{1,0:T(8,128)} %param.10) | copy-start | bytes 786436
  30.9 73.7 %all-reduce.2.cloned.1.call-start = ((), (), s32[]{:S(2)}) async-start(), calls=%async_computation.2 | async-start | bytes 524288 | tf_op jit(solution)/shard_map/psum | solution.py:24
  60.1 74.7 %all-gather.2.cloned.1.call-start = ((), (), s32[]{:S(2)}) async-start(), calls=%async_computation.3 | async-start | bytes 1310720 | tf_op jit(solution)/shard_map/all_gather | solution.py:28
  106.6 28.2 %copy-start.2 = (bf16[512,128]{1,0:T(8,128)(2,1)S(1)}, bf16[512,128]{1,0:T(8,128)(2,1)}, u32[]{:S(2)}) copy-start(bf16[512,128]{1,0:T(8,128)(2,1)} %param.8) | copy-start | bytes 393220
  172.7 5.4 %copy-start.1 = (f32[32,2048]{1,0:T(8,128)S(1)}, f32[32,2048]{1,0:T(8,128)}, u32[]{:S(2)}) copy-start(f32[32,2048]{1,0:T(8,128)} %all-reduce.2.cloned.1.call-done) | copy-start | bytes 786436
Sparse Core Ops, SparseCore 0:
  31.0 29.0 reduce-scatter.1
  63.0 41.5 all-reduce.1
  106.8 27.9 all-gather.1
where the time goes:
time: 186 us; the launch traced here: 185 us
  waiting for transfers between devices  96.5 us (52%)
  blocking collectives  33 us (18%)
  local copies, waits for them, and re-layouts  19.2 us (10%)
  between operations  14.5 us (8%)
  matrix products  11.9 us (6%)
  other arithmetic  10.2 us (5%)
    psum x1, waiting for transfers between devices, on_device(): low_grad = lax.psum(low_grad, 'rep')  44.5 us
    reduce_scatter x1, waiting for transfers between devices, on_device(): lax.psum_scatter(high_part + low_part, 'fs', scatter_dimension=0, tiled=T...  29.2 us
    all_gather x1, waiting for transfers between devices, on_device(): ratio_whole = lax.all_gather(ratio, 'fs', axis=0, tiled=True)  22.8 us
    unnamed x15, local copies, waits for them, and re-layouts  19.2 us
    all_gather x1, blocking collectives, on_device(): factor_whole = lax.all_gather(factor, 'fs', axis=0, tiled=True)  17.7 us
    psum x1, blocking collectives, on_device(): total = lax.psum(jnp.sum(raw * raw), ('fs', 'tp'))  15.3 us
    convert_element_type x1, other arithmetic, on_device(): new_weight.astype(jnp.bfloat16)  8.28 us
    dot_general x1, matrix products, on_device(): raw = jnp.dot(factor_wide, ratio_whole, precision=lax.Precision.HIGHEST)  5.95 us
  transfers between devices with their start and end apart: 3, of which 3 were waited for; matrix products, arithmetic and copies ran while one was open for 3% of the time, Pallas kernels for 0%

commit v1 on v0

--- a/solution.py
+++ b/solution.py
@@ -25,7 +25,12 @@
     new_first = first_decay * first_moment + (1.0 - first_decay) * low_grad
     new_second = second_decay * second_moment + (1.0 - second_decay) * low_grad * low_grad
     ratio = new_first / (jnp.sqrt(new_second) + epsilon)
-    ratio_whole = lax.all_gather(ratio, "fs", axis=0, tiled=True)
+    ring = [ratio]
+    for hop in range(3):
+        ring.append(lax.ppermute(ring[-1], "fs", [(dev, (dev + 1) % 4) for dev in range(4)]))
+    ratio_whole = jnp.roll(
+        jnp.concatenate(ring[::-1], axis=0), (lax.axis_index("fs") + 1) * ring[0].shape[0], axis=0
+    )
     raw = jnp.dot(factor_wide, ratio_whole, precision=lax.Precision.HIGHEST)
     total = lax.psum(jnp.sum(raw * raw), ("fs", "tp"))
     spread = jnp.sqrt(total / (D * E))

time: 186 us -> 182 us (0.978)
  waiting for transfers between devices: 96.5 us -> 92.9 us
    all_gather x1 -> x0, waiting for transfers between devices: 22.8 us -> none  [on_device(): ratio_whole = lax.all_gather(ratio, 'fs', axis=0, tiled=True)]
    ppermute x0 -> x3, waiting for transfers between devices: none -> 19.2 us  [on_device(): lax.ppermute(ring[-1], 'fs', [(dev, (dev + 1) % 4) for dev in range(4)])]
    unnamed x15 -> x22, local copies, waits for them, and re-layouts: 19.2 us -> 19.3 us
  transfers between devices with their start and end apart: 3 -> 5, of which waited for: 3 -> 5; matrix products, arithmetic and copies ran while one was open for 3% -> 3% of each run, Pallas kernels for 0% -> 0%
where the time goes in v1:
time: 182 us; the launch traced here: 181 us
  waiting for transfers between devices  92.9 us (51%)
  blocking collectives  31.8 us (17%)
  local copies, waits for them, and re-layouts  19.3 us (11%)
  between operations  14.8 us (8%)
  matrix products  10.8 us (6%)
  other arithmetic  10.2 us (6%)
    psum x1, waiting for transfers between devices, on_device(): low_grad = lax.psum(low_grad, 'rep')  44.5 us
    reduce_scatter x1, waiting for transfers between devices, on_device(): lax.psum_scatter(high_part + low_part, 'fs', scatter_dimension=0, tiled=T...  29.2 us
    unnamed x22, local copies, waits for them, and re-layouts  19.3 us
    ppermute x3, waiting for transfers between devices, on_device(): lax.ppermute(ring[-1], 'fs', [(dev, (dev + 1) % 4) for dev in range(4)])  19.2 us
    all_gather x1, blocking collectives, on_device(): factor_whole = lax.all_gather(factor, 'fs', axis=0, tiled=True)  17.6 us
    psum x1, blocking collectives, on_device(): total = lax.psum(jnp.sum(raw * raw), ('fs', 'tp'))  14.2 us
    convert_element_type x1, other arithmetic, on_device(): new_weight.astype(jnp.bfloat16)  8.28 us
    dot_general x1, matrix products, on_device(): raw = jnp.dot(factor_wide, ratio_whole, precision=lax.Precision.HIGHEST)  4.79 us
  transfers between devices with their start and end apart: 5, of which 5 were waited for; matrix products, arithmetic and copies ran while one was open for 3% of the time, Pallas kernels for 0%

profile of v1, /device:TPU:0, one launch (start us, length us, event | category | flops | bytes accessed | tf_op | source)
XLA Modules:
  0.0 181.4 jit_solution(15899201904070606418)
XLA Ops:
  7.2 0.0 reduce-scatter.2.cloned.1.call-start
  7.2 17.6 %all_gather.3 = bf16[2048,128]{1,0:T(8,128)(2,1)S(1)} all-gather(bf16[512,128]{1,0:T(8,128)(2,1)} %param.8), channel_id=1, replica_groups=mesh['fs'=4,'rep'=4,'tp'=2] {'fs'}, dimensions={0}, use_global_device_ids=true | all-gather | bytes 655360 | tf_op jit(solution)/shard_map/all_gather | solution.py:16
  24.8 3.6 %fusion.9 = f32[1024,128]{1,0:T(8,128)S(1)} fusion(bf16[1024,2048]{1,0:T(8,128)(2,1)} %param.6, bf16[2048,128]{1,0:T(8,128)(2,1)S(1)} %all_gather.3), kind=kOutput, calls=%fused_computation.24 | convolution fusion | flops 536870912 | bytes 5242880 | tf_op jit(solution)/shard_map/dot_general | solution.py:17
  28.4 0.0 copy-done
  28.4 0.7 fusion.4
  29.1 0.0 copy-start.3
  29.2 0.0 copy-start.4
  29.2 1.7 convolution_add_fusion
  30.9 0.0 reduce-scatter.2.cloned.1.call-update
  30.9 0.0 all-reduce.2.cloned.1.call-start
  31.0 29.2 %reduce-scatter.2.cloned.1.call-done = f32[32,2048]{1,0:T(8,128)} async-done(((f32[128,2048]{1,0:T(8,128)}), f32[32,2048]{1,0:T(8,128)}) %reduce-scatter.2.cloned.1.call-update) | async-done | bytes 262160 | tf_op jit(solution)/shard_map/reduce_scatter | solution.py:23
  60.1 0.0 all-reduce.2.cloned.1.call-update
  60.1 44.5 %all-reduce.2.cloned.1.call-done = f32[32,2048]{1,0:T(8,128)} async-done(((f32[32,2048]{1,0:T(8,128)}), f32[32,2048]{1,0:T(8,128)}) %all-reduce.2.cloned.1.call-update) | async-done | bytes 262160 | tf_op jit(solution)/shard_map/psum | solution.py:24
  104.6 0.0 copy-done.3
  104.6 0.0 copy-done.4
  104.6 1.9 %add_divide_fusion = (f32[32,2048]{1,0:T(8,128)S(1)}, f32[32,2048]{1,0:T(8,128)}, f32[32,2048]{1,0:T(8,128)}) fusion(f32[32,2048]{1,0:T(8,128)} %all-reduce.2.cloned.1.call-done, f32[32,2048]{1,0:T(8,128)S(1)} %copy-done.3, f32[32,2048]{1,0:T(8,128)S(1)} %copy-done.4), kind=kLoop, calls=%fused_computation.10 | loop fusion | flops 524288 | bytes 1572864 | tf_op jit(solution)/shard_map/div | solution.py:27
  106.5 1.5 collective-permute-start
  108.0 7.9 %collective-permute-done = f32[32,2048]{1,0:T(8,128)S(1)} collective-permute-done((f32[32,2048]{1,0:T(8,128)S(1)}, f32[32,2048]{1,0:T(8,128)S(1)}, u32[]{:S(2)}, u32[]{:S(2)}) %collective-permute-start) | collective-permute-done | bytes 262176 | tf_op jit(solution)/shard_map/ppermute | solution.py:30
  115.9 0.0 collective-permute-start.1
  115.9 8.5 %collective-permute-done.1 = f32[32,2048]{1,0:T(8,128)S(1)} collective-permute-done((f32[32,2048]{1,0:T(8,128)S(1)}, f32[32,2048]{1,0:T(8,128)S(1)}, u32[]{:S(2)}, u32[]{:S(2)}) %collective-permute-start.1) | collective-permute-done | bytes 262176 | tf_op jit(solution)/shard_map/ppermute | solution.py:30
  124.4 0.0 collective-permute-start.2
  124.4 5.3 %copy.12 = f32[512,2048]{0,1:T(8,128)} copy(f32[512,2048]{1,0:T(8,128)} %param.9) | data formatting | bytes 8388608 | tf_op args[3]
  129.7 2.8 %collective-permute-done.2 = f32[32,2048]{1,0:T(8,128)S(1)} collective-permute-done((f32[32,2048]{1,0:T(8,128)S(1)}, f32[32,2048]{1,0:T(8,128)S(1)}, u32[]{:S(2)}, u32[]{:S(2)}) %collective-permute-start.2) | collective-permute-done | bytes 262176 | tf_op jit(solution)/shard_map/ppermute | solution.py:30
  132.8 0.0 copy-done.2
  132.8 4.8 %multiply_reduce_fusion = (f32[]{:T(128)}, f32[2048,512]{1,0:T(8,128)}) fusion(bf16[512,128]{1,0:T(8,128)(2,1)S(1)} %copy-done.2, f32[256,2048]{1,0:T(8,128)S(1)} %constant_dynamic-update-slice_fusion, s32[]{:T(128)S(6)} %select_n.14), kind=kOutput, calls=%fused_computation.2 | convolution fusion | flops 1612709888 | bytes 5373960 | tf_op jit(solution)/shard_map/dot_general | solution.py:34
  137.6 14.2 %psum.15 = f32[]{:T(128)} all-reduce(f32[]{:T(128)} %get-tuple-element.18), channel_id=1, replica_groups=mesh['fs'=4,'rep'=4,'tp'=2] {'fs','tp'}, use_global_device_ids=true, to_apply=%region_3.4 | all-reduce | flops 1 | bytes 8 | tf_op jit(solution)/shard_map/psum | solution.py:35
  152.5 8.3 %fusion.7 = (bf16[512,2048]{0,1:T(8,128)(2,1)S(1)}, f32[512,2048]{0,1:T(8,128)}, f32[512,2048]{0,1:T(8,128)}) fusion(f32[512,2048]{0,1:T(8,128)} %copy.12, f32[2048,512]{1,0:T(8,128)} %get-tuple-element.19, f32[]{:T(128)S(6)} %add.45), kind=kLoop, calls=%fused_computation.23 | loop fusion | flops 4194304 | bytes 18874372 | tf_op jit(solution)/shard_map/convert_element_type | solution.py:39
  160.8 2.4 %copy.15 = bf16[512,2048]{1,0:T(8,128)(2,1)} copy(bf16[512,2048]{0,1:T(8,128)(2,1)S(1)} %get-tuple-element.12) | data formatting | bytes 4194304
  163.1 5.3 %copy.14 = f32[512,2048]{1,0:T(8,128)} copy(f32[512,2048]{0,1:T(8,128)} %get-tuple-element.13) | data formatting | bytes 8388608
  168.5 5.4 %copy.13 = f32[512,2048]{1,0:T(8,128)} copy(f32[512,2048]{0,1:T(8,128)} %get-tuple-element.14) | data formatting | bytes 8388608
  173.9 0.0 copy-done.1
  173.9 0.7 copy.24
  (11 shorter events, 0.2 us)
Async XLA Ops:
  7.2 53.0 %reduce-scatter.2.cloned.1.call-start = ((), (), s32[]{:S(2)}) async-start(), calls=%async_computation.1 | async-start | bytes 1310720 | tf_op jit(solution)/shard_map/reduce_scatter | solution.py:23
  24.8 3.6 %copy-start = (bf16[1024,2048]{1,0:T(8,128)(2,1)S(1)}, bf16[1024,2048]{1,0:T(8,128)(2,1)}, u32[]{:S(2)}) copy-start(bf16[1024,2048]{1,0:T(8,128)(2,1)} %param.7) | copy-start | bytes 12582916
  29.1 75.5 %copy-start.3 = (f32[32,2048]{1,0:T(8,128)S(1)}, f32[32,2048]{1,0:T(8,128)}, u32[]{:S(2)}) copy-start(f32[32,2048]{1,0:T(8,128)} %param.11) | copy-start | bytes 786436
  29.2 75.5 %copy-start.4 = (f32[32,2048]{1,0:T(8,128)S(1)}, f32[32,2048]{1,0:T(8,128)}, u32[]{:S(2)}) copy-start(f32[32,2048]{1,0:T(8,128)} %param.10) | copy-start | bytes 786436
  30.9 73.7 %all-reduce.2.cloned.1.call-start = ((), (), s32[]{:S(2)}) async-start(), calls=%async_computation.2 | async-start | bytes 524288 | tf_op jit(solution)/shard_map/psum | solution.py:24
  106.5 9.4 %collective-permute-start = (f32[32,2048]{1,0:T(8,128)S(1)}, f32[32,2048]{1,0:T(8,128)S(1)}, u32[]{:S(2)}, u32[]{:S(2)}) collective-permute-start(f32[32,2048]{1,0:T(8,128)S(1)} %get-tuple-element.15), channel_id=1, source_target_pairs={{0,8},{8,16},{16,24},{24,0},{1,9},{9,17},{17,25},{25,1},{2,10},{10... | collective-permute-start | bytes 786440 | tf_op jit(solution)/shard_map/ppermute | solution.py:30
  115.9 8.5 %collective-permute-start.1 = (f32[32,2048]{1,0:T(8,128)S(1)}, f32[32,2048]{1,0:T(8,128)S(1)}, u32[]{:S(2)}, u32[]{:S(2)}) collective-permute-start(f32[32,2048]{1,0:T(8,128)S(1)} %collective-permute-done), channel_id=1, source_target_pairs={{0,8},{8,16},{16,24},{24,0},{1,9},{9,17},{17,25},{25,1},{2,10},{10... | collective-permute-start | bytes 786440 | tf_op jit(solution)/shard_map/ppermute | solution.py:30
  124.4 8.2 %collective-permute-start.2 = (f32[32,2048]{1,0:T(8,128)S(1)}, f32[32,2048]{1,0:T(8,128)S(1)}, u32[]{:S(2)}, u32[]{:S(2)}) collective-permute-start(f32[32,2048]{1,0:T(8,128)S(1)} %collective-permute-done.1), channel_id=1, source_target_pairs={{0,8},{8,16},{16,24},{24,0},{1,9},{9,17},{17,25},{25,1},{2,10},{10... | collective-permute-start | bytes 786440 | tf_op jit(solution)/shard_map/ppermute | solution.py:30
  129.7 3.0 %copy-start.2 = (bf16[512,128]{1,0:T(8,128)(2,1)S(1)}, bf16[512,128]{1,0:T(8,128)(2,1)}, u32[]{:S(2)}) copy-start(bf16[512,128]{1,0:T(8,128)(2,1)} %param.8) | copy-start | bytes 393220
  168.5 5.4 %copy-start.1 = (f32[32,2048]{1,0:T(8,128)S(1)}, f32[32,2048]{1,0:T(8,128)}, u32[]{:S(2)}) copy-start(f32[32,2048]{1,0:T(8,128)} %all-reduce.2.cloned.1.call-done) | copy-start | bytes 786436
Sparse Core Ops, SparseCore 0:
  31.0 29.0 reduce-scatter.1
  63.0 41.5 all-reduce.1
